TPU v7x, 128 devices: a whole 4x4x4 slice. The times are simulated.
128 devices in a mesh: ep: 128 (over z, y, x, core).
Axes of the slice: x: 4, y: 4, z: 4, core: 2. Of those that a mesh axis runs over, the one named last changes fastest.
Arguments:
- residual_in: bfloat16 [1024, 2048], P('ep'), may hold values from -6 to 6
- gain_mix_pre: float32 [2048], replicated, may hold values from 0.1 to 1.9
- w_query: bfloat16 [2048, 2048], P(None, 'ep'), may hold values from -0.125 to 0.125
- w_key: bfloat16 [2048, 2048], P(None, 'ep'), may hold values from -0.125 to 0.125
- w_value: bfloat16 [2048, 2048], P(None, 'ep'), may hold values from -0.125 to 0.125
- w_outgate: bfloat16 [2048, 2048], P(None, 'ep'), may hold values from -0.125 to 0.125
- w_decay: bfloat16 [2048, 16], replicated, may hold values from -0.125 to 0.125
- w_beta: bfloat16 [2048, 16], replicated, may hold values from -0.125 to 0.125
- decay_scale: float32 [16], replicated, may hold values from 1 to 16
- decay_bias: float32 [16], replicated, may hold values from -5 to -1
- head_gain: float32 [128], replicated, may hold values from 0.1 to 1.9
- w_out: bfloat16 [2048, 2048], replicated, may hold values from -0.125 to 0.125
- gain_mix_post: float32 [2048], replicated, may hold values from 0.1 to 1.9
- state_cache: bfloat16 [1024, 16, 128, 128], P('ep'), may hold values from -2.390625 to 2.390625
- gain_ffn_pre: float32 [2048], replicated, may hold values from 0.1 to 1.9
- routes: int32 [1024, 4], P('ep'), may hold values from 0 to 31, all different within a row; in each aligned block of 8 rows (0 to 7, 8 to 15, ...) at most 2 rows name the same one
- route_logits: float32 [1024, 4], P('ep'), may hold values from -6 to 6
- w_gate: bfloat16 [2048, 65536], P(None, 'ep'), may hold values from -0.375 to 0.375
- w_up: bfloat16 [2048, 65536], P(None, 'ep'), may hold values from -0.375 to 0.375
- w_down: bfloat16 [65536, 2048], P('ep'), may hold values from -0.125 to 0.125
- gain_ffn_post: float32 [2048], replicated, may hold values from 0.1 to 1.9
Outputs:
- result: bfloat16 [1024, 2048], P('ep')
- new_state: bfloat16 [1024, 16, 128, 128], P('ep')
Inputs may be any that keep to these rules, and one draw needn't show every extreme that they name: `routes`: each row names 4 different experts. In the rows of one device (aligned blocks of 8 rows) no expert is named more than 2 times, and in some block one expert is named exactly 2 times.
All inputs are finite; a program needn't handle non-finite values.
Results may differ from a plain program's by a relative error of at most 0.014.
Values may be sent and summed in bfloat16 or wider, within the bound.
No kernel may reach another device: no remote copies, remote signals or barrier semaphores. Data moves between devices by JAX's collectives and lax.ppermute only.
A program may use at most 128 MiB of HBM per device.

v0:
```python
import jax
import jax.numpy as jnp
from jax import lax
from jax.sharding import PartitionSpec as P

H = 16
HD = 128
PIECES = 4
TOPK = 4
EPS = 1e-06
LIMIT = 7.0
ALPHA = 1.702


def rms_scale(values):
    return values * lax.rsqrt(jnp.mean(values * values, axis=-1, keepdims=True) + EPS)


def clamped_unit(gate, upper):
    glu = jnp.minimum(gate, LIMIT)
    linear = jnp.clip(upper, -LIMIT, LIMIT)
    return glu * jax.nn.sigmoid(ALPHA * glu) * (linear + 1.0)


def dispatch_table(routes, experts, capacity):
    count, topk = routes.shape
    hits = (routes[:, :, None] == jnp.arange(experts, dtype=jnp.int32)).astype(jnp.int32)
    flat = hits.reshape(count * topk, experts)
    before = jnp.cumsum(flat, axis=0) - flat
    slots = jnp.sum(before * flat, axis=1).reshape(count, topk)
    target = routes * capacity + slots
    return (target[:, :, None] == jnp.arange(experts * capacity, dtype=jnp.int32)).astype(
        jnp.float32
    )


def delta_step(
    q_raw, k_raw, v_raw, z_raw, decay_in, beta_in, state, decay_scale, decay_bias, head_gain
):
    count = q_raw.shape[0]
    query = jax.nn.silu(q_raw.astype(jnp.float32)).reshape(count, H, HD)
    query = query * lax.rsqrt(jnp.sum(query * query, axis=-1, keepdims=True) + EPS) * HD ** (-0.5)
    keys = jax.nn.silu(k_raw.astype(jnp.float32)).reshape(count, H, HD)
    keys = keys * lax.rsqrt(jnp.sum(keys * keys, axis=-1, keepdims=True) + EPS)
    values = jax.nn.silu(v_raw.astype(jnp.float32)).reshape(count, H, HD)
    decay = -decay_scale * jax.nn.softplus(decay_in + decay_bias)
    beta = jax.nn.sigmoid(beta_in)
    held = state.astype(jnp.float32) * jnp.exp(decay)[:, :, None, None]
    guess = jnp.einsum("rhk,rhkv->rhv", keys, held)
    held = held + jnp.einsum("rhk,rhv->rhkv", keys, beta[:, :, None] * (values - guess))
    output = jnp.einsum("rhk,rhkv->rhv", query, held)
    output = rms_scale(output) * head_gain
    gated = output.reshape(count, H * HD) * jax.nn.silu(z_raw.astype(jnp.float32))
    return (gated.astype(jnp.bfloat16), held.astype(jnp.bfloat16))


def shards(
    residual_in,
    gain_mix_pre,
    w_query,
    w_key,
    w_value,
    w_outgate,
    w_decay,
    w_beta,
    decay_scale,
    decay_bias,
    head_gain,
    w_out,
    gain_mix_post,
    state_cache,
    gain_ffn_pre,
    routes,
    route_logits,
    w_gate,
    w_up,
    w_down,
    gain_ffn_post,
):
    devices = lax.axis_size("ep")
    count, width = residual_in.shape
    x_first = residual_in.astype(jnp.float32)
    normed = (rms_scale(x_first) * gain_mix_pre).astype(jnp.bfloat16)
    stacked = jnp.stack([w_query, w_key, w_value, w_outgate])
    columns = jnp.einsum(
        "td,rdc->trc",
        lax.all_gather(normed, "ep", axis=0, tiled=True),
        stacked,
        preferred_element_type=jnp.float32,
    ).astype(jnp.bfloat16)
    joined = lax.all_to_all(columns, "ep", split_axis=0, concat_axis=2, tiled=True)
    decay_in = jnp.dot(normed, w_decay, preferred_element_type=jnp.float32)
    beta_in = jnp.dot(normed, w_beta, preferred_element_type=jnp.float32)
    mixed, new_state = delta_step(
        joined[:, 0],
        joined[:, 1],
        joined[:, 2],
        joined[:, 3],
        decay_in,
        beta_in,
        state_cache,
        decay_scale,
        decay_bias,
        head_gain,
    )
    branch = jnp.dot(mixed, w_out, preferred_element_type=jnp.float32)
    x_second = x_first + rms_scale(branch) * gain_mix_post
    normed_two = (rms_scale(x_second) * gain_ffn_pre).astype(jnp.bfloat16)
    experts = devices // PIECES
    capacity = max(2, 2 * count * TOPK // experts)
    table = dispatch_table(routes, experts, capacity)
    picks = jnp.sum(table, axis=1).astype(jnp.bfloat16)
    sent = lax.dot_general(
        picks, normed_two, (((0,), (0,)), ((), ())), preferred_element_type=jnp.float32
    ).astype(jnp.bfloat16)
    sent = jnp.broadcast_to(
        sent.reshape(experts, 1, capacity, width), (experts, PIECES, capacity, width)
    ).reshape(devices, capacity, width)
    block = lax.all_to_all(sent, "ep", split_axis=0, concat_axis=0, tiled=True)
    flat = block.reshape(-1, width)
    hidden = clamped_unit(
        jnp.dot(flat, w_gate, preferred_element_type=jnp.float32),
        jnp.dot(flat, w_up, preferred_element_type=jnp.float32),
    ).astype(jnp.bfloat16)
    partial_value = jnp.dot(hidden, w_down, preferred_element_type=jnp.float32).astype(jnp.bfloat16)
    returned = lax.all_to_all(
        partial_value.reshape(block.shape), "ep", split_axis=0, concat_axis=0, tiled=True
    )
    summed = jnp.sum(returned.reshape(experts, PIECES, capacity, width).astype(jnp.float32), axis=1)
    summed = summed.reshape(experts * capacity, width)
    raised = jnp.exp(route_logits)
    weights = raised / jnp.sum(raised, axis=-1, keepdims=True)
    mix_table = jnp.einsum("ske,sk->se", table, weights)
    moe = jnp.dot(mix_table, summed)
    result = (x_second + rms_scale(moe) * gain_ffn_post).astype(jnp.bfloat16)
    return (result, new_state)


def solution(mesh):
    in_specs = (
        P("ep", None),
        P(),
        P(None, "ep"),
        P(None, "ep"),
        P(None, "ep"),
        P(None, "ep"),
        P(),
        P(),
        P(),
        P(),
        P(),
        P(),
        P(),
        P("ep", None, None, None),
        P(),
        P("ep", None),
        P("ep", None),
        P(None, "ep"),
        P(None, "ep"),
        P("ep", None),
        P(),
    )
    out_specs = (P("ep", None), P("ep", None, None, None))
    return jax.shard_map(shards, mesh=mesh, in_specs=in_specs, out_specs=out_specs, check_vma=False)
```

profile of v0, /device:TPU:1, one launch (start us, length us, event | category | flops | bytes accessed | tf_op | source)
XLA Modules:
  0.0 186.9 jit_solution(18092461676442256661)
XLA Ops:
  7.2 1.0 fusion.38
  8.3 1.5 fusion.40
  11.6 1.0 fusion.12
  12.6 1.0 fusion.57
  14.6 67.3 %all-gather.2.cloned.1.call-done = bf16[1024,2048]{1,0:T(8,128)(2,1)} async-done(((bf16[8,2048]{1,0:T(8,128)(2,1)}), bf16[1024,2048]{1,0:T(8,128)(2,1)}) %all-gather.2.cloned.1.call-update) | async-done | bytes 4194320 | tf_op jit(solution)/shard_map/all_gather | solution.py:87
  81.9 3.6 %fusion.65 = f32[1024,64]{0,1:S(1)} fusion(bf16[1024,2048]{1,0:T(8,128)(2,1)} %all-gather.2.cloned.1.call-done, bf16[2048,64]{0,1:T(8,128)(2,1)S(1)} %bitcast.103), kind=kOutput, calls=%fused_computation.116 | convolution fusion | flops 268435456 | bytes 4718592
  86.2 1.5 reshape.127
  87.7 5.5 %all-to-all-start = ((bf16[128,2,256]{2,1,0:T(2,128)(2,1)}), bf16[128,2,256]{2,1,0:T(2,128)(2,1)S(1)}, u32[]{:S(2)}, u32[]{:S(2)}) async-start(bf16[128,2,256]{2,1,0:T(2,128)(2,1)} %reshape.127), calls=%async_computation | async-start | bytes 262144 | tf_op jit(solution)/shard_map/all_to_all | solution.py:91
  93.5 9.8 %all-to-all-done = bf16[128,2,256]{2,1,0:T(2,128)(2,1)S(1)} async-done(((bf16[128,2,256]{2,1,0:T(2,128)(2,1)}), bf16[128,2,256]{2,1,0:T(2,128)(2,1)S(1)}, u32[]{:S(2)}, u32[]{:S(2)}) %all-to-all-start) | async-done | bytes 131104 | tf_op jit(solution)/shard_map/all_to_all | solution.py:91
  104.3 1.8 all_to_all.22
  106.4 3.6 %fusion = f32[8,16,1,128]{3,2,1,0:T(1,128)S(1)} fusion(bf16[8,16,128,128]{3,2,1,0:T(8,128)(2,1)} %param.34, f32[8,16]{1,0:T(8,128)S(1)} %fusion.57, bf16[8,16,128,1]{2,0,1,3:T(8,128)(2,1)S(1)} %get-tuple-element.5), kind=kOutput, calls=%fused_computation.2 | convolution fusion | flops 8388608 | bytes 4293120 | tf_op jit(solution)/shard_map/rhk,rhkv->rhv/dot_general | solution.py:49
  110.2 3.8 %fusion.2 = f32[8,16,1,128]{3,2,1,0:T(1,128)S(1)} fusion(bf16[8,16,128,128]{3,2,1,0:T(8,128)(2,1)S(1)} %copy-done.1, f32[8,16,128]{2,1,0:T(8,128)S(1)} %copy.46, f32[8,16,128]{2,1,0:T(8,128)S(1)} %copy.44, f32[8,16]{1,0:T(8,128)S(1)} %fusion.57, bf16[8,16,128,1]{2,0,1,3:T(8,128)(2,1)S(1)} %get-tuple-element.4), kind=kOutput, calls=%fused_computation.4 | convolution fusion | flops 12582912 | bytes 4424192 | tf_op jit(solution)/shard_map/rhk,rhkv->rhv/dot_general | solution.py:51
  114.1 4.7 %multiply_reduce_fusion.2 = (f32[8]{0:T(128)S(1)}, f32[8,2048]{1,0:T(8,128)S(1)}) fusion(bf16[2048,2048]{1,0:T(8,128)(2,1)} %param.32, f32[8,16,1,128]{3,2,1,0:T(1,128)S(1)} %fusion.2, bf16[8,4,2048]{2,0,1:T(8,128)(2,1)S(1)} %all_to_all.22, f32[128]{0:T(128)S(1)} %copy-done.7, f32[8,16]{0,1:T(8,128)S(1)} %add_rsqrt_fusion), kind=kOutput, calls=%fused_computation.73 | convolution fusion | flops 67289080 | bytes 8561184 | tf_op jit(solution)/shard_map/dot_general | solution.py:106
  119.6 1.6 broadcast_in_dim.5
  121.2 4.2 %all-to-all-start.1 = ((bf16[128,2,2048]{2,1,0:T(2,128)(2,1)}), bf16[128,2,2048]{2,1,0:T(2,128)(2,1)S(1)}, u32[]{:S(2)}, u32[]{:S(2)}) async-start(bf16[128,2,2048]{2,1,0:T(2,128)(2,1)} %bitcast.25), calls=%async_computation.1 | async-start | bytes 2097152 | tf_op jit(solution)/shard_map/all_to_all | solution.py:119
  125.5 19.2 %all-to-all-done.1 = bf16[128,2,2048]{2,1,0:T(2,128)(2,1)S(1)} async-done(((bf16[128,2,2048]{2,1,0:T(2,128)(2,1)}), bf16[128,2,2048]{2,1,0:T(2,128)(2,1)S(1)}, u32[]{:S(2)}, u32[]{:S(2)}) %all-to-all-start.1) | async-done | bytes 1048608 | tf_op jit(solution)/shard_map/all_to_all | solution.py:119
  144.7 1.2 reshape.111
  145.9 3.4 %convolution_minimum_fusion = f32[256,512]{1,0:T(8,128)} fusion(bf16[256,2048]{1,0:T(8,128)(2,1)} %reshape.111, bf16[2048,512]{1,0:T(8,128)(2,1)} %param.38), kind=kOutput, calls=%fused_computation.13 | convolution fusion | flops 537001984 | bytes 3670016 | tf_op jit(solution)/shard_map/dot_general | solution.py:122
  149.3 3.4 %convolution_convert_fusion = bf16[256,2048]{1,0:T(8,128)(2,1)S(1)} fusion(bf16[512,2048]{1,0:T(8,128)(2,1)S(1)} %copy-done, bf16[256,2048]{1,0:T(8,128)(2,1)} %reshape.111, bf16[2048,512]{1,0:T(8,128)(2,1)} %param.39, f32[256,512]{1,0:T(8,128)} %convolution_minimum_fusion), kind=kOutput, calls=%fused_computation.9 | convolution fusion | flops 1075445760 | bytes 6815744 | tf_op jit(solution)/shard_map/dot_general | solution.py:125
  152.6 1.5 reshape.112
  154.2 4.4 %all-to-all-start.2 = ((bf16[128,2,2048]{2,1,0:T(2,128)(2,1)}), bf16[128,2,2048]{2,1,0:T(2,128)(2,1)S(1)}, u32[]{:S(2)}, u32[]{:S(2)}) async-start(bf16[128,2,2048]{2,1,0:T(2,128)(2,1)} %reshape.112), calls=%async_computation.2 | async-start | bytes 2097152 | tf_op jit(solution)/shard_map/all_to_all | solution.py:126
  158.9 6.0 %fusion.1 = bf16[8,16,128,128]{3,2,1,0:T(8,128)(2,1)} fusion(bf16[8,16,128,128]{3,2,1,0:T(8,128)(2,1)} %param.34, f32[8,16,128]{2,1,0:T(8,128)S(1)} %copy.46, f32[8,16,128]{2,1,0:T(8,128)S(1)} %copy.44, f32[8,16]{1,0:T(8,128)S(1)} %fusion.57), kind=kLoop, calls=%fused_computation.3 | loop fusion | flops 10485760 | bytes 8520192 | tf_op jit(solution)/shard_map/convert_element_type | solution.py:54
  164.9 13.0 %all-to-all-done.2 = bf16[128,2,2048]{2,1,0:T(2,128)(2,1)S(1)} async-done(((bf16[128,2,2048]{2,1,0:T(2,128)(2,1)}), bf16[128,2,2048]{2,1,0:T(2,128)(2,1)S(1)}, u32[]{:S(2)}, u32[]{:S(2)}) %all-to-all-start.2) | async-done | bytes 1048608 | tf_op jit(solution)/shard_map/all_to_all | solution.py:126
  177.9 1.0 convert_reduce_fusion
  (58 shorter events, 7.6 us)
Async XLA Ops:
  7.2 142.1 %copy-start = (bf16[512,2048]{1,0:T(8,128)(2,1)S(1)}, bf16[512,2048]{1,0:T(8,128)(2,1)}, u32[]{:S(2)}) copy-start(bf16[512,2048]{1,0:T(8,128)(2,1)} %param.40) | copy-start | bytes 6291460
  7.2 74.7 %all-gather.2.cloned.1.call-start = ((), (), s32[]{:S(2)}) async-start(), calls=%async_computation.3 | async-start | bytes 4227072 | tf_op jit(solution)/shard_map/all_gather | solution.py:87
  87.7 15.5 %all-to-all-start = ((bf16[128,2,256]{2,1,0:T(2,128)(2,1)}), bf16[128,2,256]{2,1,0:T(2,128)(2,1)S(1)}, u32[]{:S(2)}, u32[]{:S(2)}) async-start(bf16[128,2,256]{2,1,0:T(2,128)(2,1)} %reshape.127), calls=%async_computation | async-start | bytes 262144 | tf_op jit(solution)/shard_map/all_to_all | solution.py:91
  106.1 4.0 %copy-start.1 = (bf16[8,16,128,128]{3,2,1,0:T(8,128)(2,1)S(1)}, bf16[8,16,128,128]{3,2,1,0:T(8,128)(2,1)}, u32[]{:S(2)}) copy-start(bf16[8,16,128,128]{3,2,1,0:T(8,128)(2,1)} %param.34) | copy-start | bytes 12582916
  110.2 3.9 %copy-start.7 = (f32[128]{0:T(128)S(1)}, f32[128]{0:T(128)}, u32[]{:S(2)}) copy-start(f32[128]{0:T(128)} %param.31) | copy-start | bytes 1540
  114.1 4.8 %copy-start.2 = (bf16[8,2048]{1,0:T(8,128)(2,1)S(1)}, bf16[8,2048]{1,0:T(8,128)(2,1)}, u32[]{:S(2)}) copy-start(bf16[8,2048]{1,0:T(8,128)(2,1)} %param.21) | copy-start | bytes 98308
  114.1 4.8 %copy-start.3 = (f32[2048]{0:T(1024)S(1)}, f32[2048]{0:T(1024)}, u32[]{:S(2)}) copy-start(f32[2048]{0:T(1024)} %param.33) | copy-start | bytes 24580
  114.1 5.0 %copy-start.4 = (f32[2048]{0:T(1024)S(1)}, f32[2048]{0:T(1024)}, u32[]{:S(2)}) copy-start(f32[2048]{0:T(1024)} %param.35) | copy-start | bytes 24580
  118.9 6.6 %copy-start.5 = (f32[8,4]{0,1:T(4,128)S(1)}, f32[8,4]{0,1:T(4,128)}, u32[]{:S(2)}) copy-start(f32[8,4]{0,1:T(4,128)} %param.37) | copy-start | bytes 388
  121.2 23.4 %all-to-all-start.1 = ((bf16[128,2,2048]{2,1,0:T(2,128)(2,1)}), bf16[128,2,2048]{2,1,0:T(2,128)(2,1)S(1)}, u32[]{:S(2)}, u32[]{:S(2)}) async-start(bf16[128,2,2048]{2,1,0:T(2,128)(2,1)} %bitcast.25), calls=%async_computation.1 | async-start | bytes 2097152 | tf_op jit(solution)/shard_map/all_to_all | solution.py:119
  154.2 23.8 %all-to-all-start.2 = ((bf16[128,2,2048]{2,1,0:T(2,128)(2,1)}), bf16[128,2,2048]{2,1,0:T(2,128)(2,1)S(1)}, u32[]{:S(2)}, u32[]{:S(2)}) async-start(bf16[128,2,2048]{2,1,0:T(2,128)(2,1)} %reshape.112), calls=%async_computation.2 | async-start | bytes 2097152 | tf_op jit(solution)/shard_map/all_to_all | solution.py:126
  158.9 20.4 %copy-start.6 = (f32[2048]{0:T(1024)S(1)}, f32[2048]{0:T(1024)}, u32[]{:S(2)}) copy-start(f32[2048]{0:T(1024)} %param.41) | copy-start | bytes 24580
Sparse Core Ops, SparseCore 0:
  11.7 70.1 all-gather.1
where the time goes:
time: 188 us; the launch traced here: 187 us
  waiting for transfers between devices  109 us (58%)
  matrix products  25.2 us (13%)
  between operations  14.3 us (8%)
  starting transfers between devices  14.2 us (8%)
  other arithmetic  13 us (7%)
  local copies, waits for them, and re-layouts  10.9 us (6%)
    all_gather x1, waiting for transfers between devices, shards(): lax.all_gather(normed, 'ep', axis=0, tiled=True)  67.3 us
    all_to_all x1, waiting for transfers between devices, shards(): block = lax.all_to_all(sent, 'ep', split_axis=0, concat_axis=0, tiled=True)  19.2 us
    all_to_all x1, waiting for transfers between devices, shards(): lax.all_to_all(partial_value.reshape(block.shape), 'ep', split_axis=0, co...  13 us
    all_to_all x1, waiting for transfers between devices, shards(): lax.all_to_all(columns, 'ep', split_axis=0, concat_axis=2, tiled=True)  9.77 us
    convert_element_type x1, other arithmetic, delta_step(): return (gated.astype(jnp.bfloat16), held.astype(jnp.bfloat16))  5.96 us
    all_to_all x1, starting transfers between devices, shards(): lax.all_to_all(columns, 'ep', split_axis=0, concat_axis=2, tiled=True)  5.51 us
    dot_general x1, matrix products, shards(): branch = jnp.dot(mixed, w_out, preferred_element_type=jnp.float32)  4.73 us
    all_to_all x1, starting transfers between devices, shards(): lax.all_to_all(partial_value.reshape(block.shape), 'ep', split_axis=0, co...  4.43 us
  transfers between devices with their start and end apart: 4, of which 4 were waited for; matrix products, arithmetic and copies ran while one was open for 6% of the time, Pallas kernels for 0%

commit v1 on v0

--- a/solution.py
+++ b/solution.py
@@ -10,6 +10,11 @@
 EPS = 1e-06
 LIMIT = 7.0
 ALPHA = 1.702
+
+
+def exchange_gather(array, mesh_axis, dim):
+    stack = jnp.stack([array] * lax.axis_size(mesh_axis))
+    return jnp.concatenate(lax.all_to_all(stack, mesh_axis, 0, 0), axis=dim)
 
 
 def rms_scale(values):
@@ -83,10 +88,7 @@
     normed = (rms_scale(x_first) * gain_mix_pre).astype(jnp.bfloat16)
     stacked = jnp.stack([w_query, w_key, w_value, w_outgate])
     columns = jnp.einsum(
-        "td,rdc->trc",
-        lax.all_gather(normed, "ep", axis=0, tiled=True),
-        stacked,
-        preferred_element_type=jnp.float32,
+        "td,rdc->trc", exchange_gather(normed, "ep", 0), stacked, preferred_element_type=jnp.float32
     ).astype(jnp.bfloat16)
     joined = lax.all_to_all(columns, "ep", split_axis=0, concat_axis=2, tiled=True)
     decay_in = jnp.dot(normed, w_decay, preferred_element_type=jnp.float32)

time: 188 us -> 167 us (0.89)
  waiting for transfers between devices: 109 us -> 93.7 us
  between operations: 14.3 us -> 1.07 us
  starting transfers between devices: 14.2 us -> 25 us
  other arithmetic: 13 us -> 10.8 us
  local copies, waits for them, and re-layouts: 10.9 us -> 12.8 us
    all_gather x1 -> x0, waiting for transfers between devices: 67.3 us -> none  [shards(): lax.all_gather(normed, 'ep', axis=0, tiled=True)]
    all_to_all x0 -> x1, waiting for transfers between devices: none -> 51.6 us  [exchange_gather(): return jnp.concatenate(lax.all_to_all(stack, mesh_axis, 0, 0), axis=dim)]
    all_to_all x0 -> x1, starting transfers between devices: none -> 12 us  [exchange_gather(): return jnp.concatenate(lax.all_to_all(stack, mesh_axis, 0, 0), axis=dim)]
    another operation x0 -> x1, local copies, waits for them, and re-layouts: none -> 2.54 us  [exchange_gather(): stack = jnp.stack([array] * lax.axis_size(mesh_axis))]
  transfers between devices with their start and end apart: 4 -> 4, of which waited for: 4 -> 4; matrix products, arithmetic and copies ran while one was open for 6% -> 4% of each run, Pallas kernels for 0% -> 0%
where the time goes in v1:
time: 167 us
  waiting for transfers between devices  93.7 us (56%)
  starting transfers between devices  25 us (15%)
  matrix products  23.4 us (14%)
  local copies, waits for them, and re-layouts  12.8 us (8%)
  other arithmetic  10.8 us (6%)
    all_to_all x1, waiting for transfers between devices, exchange_gather(): return jnp.concatenate(lax.all_to_all(stack, mesh_axis, 0, 0), axis=dim)  51.6 us
    all_to_all x1, waiting for transfers between devices, shards(): block = lax.all_to_all(sent, 'ep', split_axis=0, concat_axis=0, tiled=True)  19.2 us
    all_to_all x1, waiting for transfers between devices, shards(): lax.all_to_all(partial_value.reshape(block.shape), 'ep', split_axis=0, co...  13 us
    all_to_all x1, starting transfers between devices, exchange_gather(): return jnp.concatenate(lax.all_to_all(stack, mesh_axis, 0, 0), axis=dim)  12 us
    all_to_all x1, waiting for transfers between devices, shards(): lax.all_to_all(columns, 'ep', split_axis=0, concat_axis=2, tiled=True)  9.91 us
    convert_element_type x1, other arithmetic, delta_step(): return (gated.astype(jnp.bfloat16), held.astype(jnp.bfloat16))  5.96 us
    dot_general x1, matrix products, shards(): branch = jnp.dot(mixed, w_out, preferred_element_type=jnp.float32)  4.73 us
    all_to_all x1, starting transfers between devices, shards(): lax.all_to_all(partial_value.reshape(block.shape), 'ep', split_axis=0, co...  4.43 us
  transfers between devices with their start and end apart: 4, of which 4 were waited for; matrix products, arithmetic and copies ran while one was open for 4% of the time, Pallas kernels for 0%

profile of v1, /device:TPU:1, one launch (start us, length us, event | category | flops | bytes accessed | tf_op | source)
XLA Modules:
  0.0 166.9 jit_solution(10750980709047537673)
XLA Ops:
  0.6 1.0 fusion.40
  1.7 0.8 fusion.42
  2.5 2.5 %stack.12 = bf16[128,8,2048]{2,1,0:T(8,128)(2,1)} broadcast(bf16[8,2048]{1,0:T(8,128)(2,1)S(1)} %fusion.42), dimensions={1,2} | broadcast | bytes 4227072 | tf_op jit(solution)/shard_map/stack | solution.py:16
  5.1 12.0 %all-to-all-start = ((bf16[128,8,2048]{2,1,0:T(8,128)(2,1)}), bf16[128,8,2048]{2,1,0:T(8,128)(2,1)}, u32[]{:S(2)}, u32[]{:S(2)}) async-start(bf16[128,8,2048]{2,1,0:T(8,128)(2,1)} %stack.12), calls=%async_computation | async-start | bytes 8388608 | tf_op jit(solution)/shard_map/all_to_all | solution.py:17
  18.1 51.6 %all-to-all-done = bf16[128,8,2048]{2,1,0:T(8,128)(2,1)} async-done(((bf16[128,8,2048]{2,1,0:T(8,128)(2,1)}), bf16[128,8,2048]{2,1,0:T(8,128)(2,1)}, u32[]{:S(2)}, u32[]{:S(2)}) %all-to-all-start) | async-done | bytes 4194336 | tf_op jit(solution)/shard_map/all_to_all | solution.py:17
  69.7 3.6 %fusion.3 = f32[1024,64]{0,1:S(1)} fusion(bf16[2048,64]{0,1:T(8,128)(2,1)S(1)} %bitcast.105, bf16[128,8,2048]{2,1,0:T(8,128)(2,1)} %all-to-all-done), kind=kOutput, calls=%fused_computation.5 | convolution fusion | flops 268435456 | bytes 4718592
  74.0 1.5 reshape.133
  75.5 4.4 %all-to-all-start.1 = ((bf16[128,2,256]{2,1,0:T(2,128)(2,1)}), bf16[128,2,256]{2,1,0:T(2,128)(2,1)S(1)}, u32[]{:S(2)}, u32[]{:S(2)}) async-start(bf16[128,2,256]{2,1,0:T(2,128)(2,1)} %reshape.133), calls=%async_computation.1 | async-start | bytes 262144 | tf_op jit(solution)/shard_map/all_to_all | solution.py:93
  80.1 9.9 %all-to-all-done.1 = bf16[128,2,256]{2,1,0:T(2,128)(2,1)S(1)} async-done(((bf16[128,2,256]{2,1,0:T(2,128)(2,1)}), bf16[128,2,256]{2,1,0:T(2,128)(2,1)S(1)}, u32[]{:S(2)}, u32[]{:S(2)}) %all-to-all-start.1) | async-done | bytes 131104 | tf_op jit(solution)/shard_map/all_to_all | solution.py:93
  91.1 1.8 %all_to_all.26 = bf16[8,4,2048]{2,0,1:T(8,128)(2,1)S(1)} reshape(bf16[8,4,128,16]{3,2,0,1:T(8,128)(2,1)S(1)} %copy.43) | data formatting | bytes 262144 | tf_op jit(solution)/shard_map/all_to_all | solution.py:93
  93.2 3.6 %fusion = f32[8,16,1,128]{3,2,1,0:T(1,128)S(1)} fusion(bf16[8,16,128,128]{3,2,1,0:T(8,128)(2,1)} %param.34, f32[8,16]{1,0:T(8,128)S(1)} %fusion.59, bf16[8,16,128,1]{2,0,1,3:T(8,128)(2,1)S(1)} %get-tuple-element.5), kind=kOutput, calls=%fused_computation.2 | convolution fusion | flops 8388608 | bytes 4293120 | tf_op jit(solution)/shard_map/rhk,rhkv->rhv/dot_general | solution.py:54
  97.0 3.8 %fusion.2 = f32[8,16,1,128]{3,2,1,0:T(1,128)S(1)} fusion(bf16[8,16,128,128]{3,2,1,0:T(8,128)(2,1)S(1)} %copy-done.1, f32[8,16,128]{2,1,0:T(8,128)S(1)} %copy.46, f32[8,16,128]{2,1,0:T(8,128)S(1)} %copy.44, f32[8,16]{1,0:T(8,128)S(1)} %fusion.59, bf16[8,16,128,1]{2,0,1,3:T(8,128)(2,1)S(1)} %get-tuple-element.4), kind=kOutput, calls=%fused_computation.4 | convolution fusion | flops 12582912 | bytes 4424192 | tf_op jit(solution)/shard_map/rhk,rhkv->rhv/dot_general | solution.py:56
  100.9 4.7 %multiply_reduce_fusion.2 = (f32[8]{0:T(128)S(1)}, f32[8,2048]{1,0:T(8,128)S(1)}) fusion(bf16[2048,2048]{1,0:T(8,128)(2,1)} %param.32, f32[8,16,1,128]{3,2,1,0:T(1,128)S(1)} %fusion.2, bf16[8,4,2048]{2,0,1:T(8,128)(2,1)S(1)} %all_to_all.26, f32[128]{0:T(128)S(1)} %copy-done.15, f32[8,16]{0,1:T(8,128)S(1)} %add_rsqrt_fusion), kind=kOutput, calls=%fused_computation.75 | convolution fusion | flops 67289080 | bytes 8561184 | tf_op jit(solution)/shard_map/dot_general | solution.py:108
  106.4 1.6 broadcast_in_dim.5
  108.0 4.2 %all-to-all-start.2 = ((bf16[128,2,2048]{2,1,0:T(2,128)(2,1)}), bf16[128,2,2048]{2,1,0:T(2,128)(2,1)S(1)}, u32[]{:S(2)}, u32[]{:S(2)}) async-start(bf16[128,2,2048]{2,1,0:T(2,128)(2,1)} %bitcast.26), calls=%async_computation.2 | async-start | bytes 2097152 | tf_op jit(solution)/shard_map/all_to_all | solution.py:121
  112.3 19.2 %all-to-all-done.2 = bf16[128,2,2048]{2,1,0:T(2,128)(2,1)S(1)} async-done(((bf16[128,2,2048]{2,1,0:T(2,128)(2,1)}), bf16[128,2,2048]{2,1,0:T(2,128)(2,1)S(1)}, u32[]{:S(2)}, u32[]{:S(2)}) %all-to-all-start.2) | async-done | bytes 1048608 | tf_op jit(solution)/shard_map/all_to_all | solution.py:121
  131.5 1.2 reshape.117
  132.7 3.4 %convolution_minimum_fusion = f32[256,512]{1,0:T(8,128)} fusion(bf16[256,2048]{1,0:T(8,128)(2,1)} %reshape.117, bf16[2048,512]{1,0:T(8,128)(2,1)} %param.38), kind=kOutput, calls=%fused_computation.15 | convolution fusion | flops 537001984 | bytes 3670016 | tf_op jit(solution)/shard_map/dot_general | solution.py:124
  136.1 3.4 %convolution_convert_fusion = bf16[256,2048]{1,0:T(8,128)(2,1)S(1)} fusion(bf16[512,2048]{1,0:T(8,128)(2,1)S(1)} %copy-done, bf16[256,2048]{1,0:T(8,128)(2,1)} %reshape.117, bf16[2048,512]{1,0:T(8,128)(2,1)} %param.39, f32[256,512]{1,0:T(8,128)} %convolution_minimum_fusion), kind=kOutput, calls=%fused_computation.11 | convolution fusion | flops 1075445760 | bytes 6815744 | tf_op jit(solution)/shard_map/dot_general | solution.py:127
  139.4 1.5 reshape.118
  141.0 4.4 %all-to-all-start.3 = ((bf16[128,2,2048]{2,1,0:T(2,128)(2,1)}), bf16[128,2,2048]{2,1,0:T(2,128)(2,1)S(1)}, u32[]{:S(2)}, u32[]{:S(2)}) async-start(bf16[128,2,2048]{2,1,0:T(2,128)(2,1)} %reshape.118), calls=%async_computation.3 | async-start | bytes 2097152 | tf_op jit(solution)/shard_map/all_to_all | solution.py:128
  145.7 6.0 %fusion.1 = bf16[8,16,128,128]{3,2,1,0:T(8,128)(2,1)} fusion(bf16[8,16,128,128]{3,2,1,0:T(8,128)(2,1)} %param.34, f32[8,16,128]{2,1,0:T(8,128)S(1)} %copy.46, f32[8,16,128]{2,1,0:T(8,128)S(1)} %copy.44, f32[8,16]{1,0:T(8,128)S(1)} %fusion.59), kind=kLoop, calls=%fused_computation.3 | loop fusion | flops 10485760 | bytes 8520192 | tf_op jit(solution)/shard_map/convert_element_type | solution.py:59
  151.7 13.0 %all-to-all-done.3 = bf16[128,2,2048]{2,1,0:T(2,128)(2,1)S(1)} async-done(((bf16[128,2,2048]{2,1,0:T(2,128)(2,1)}), bf16[128,2,2048]{2,1,0:T(2,128)(2,1)S(1)}, u32[]{:S(2)}, u32[]{:S(2)}) %all-to-all-start.3) | async-done | bytes 1048608 | tf_op jit(solution)/shard_map/all_to_all | solution.py:128
  164.7 1.0 convert_reduce_fusion
  (76 shorter events, 5.6 us)
Async XLA Ops:
  0.6 135.4 %copy-start = (bf16[512,2048]{1,0:T(8,128)(2,1)S(1)}, bf16[512,2048]{1,0:T(8,128)(2,1)}, u32[]{:S(2)}) copy-start(bf16[512,2048]{1,0:T(8,128)(2,1)} %param.40) | copy-start | bytes 6291460
  5.1 12.0 %copy-start.16 = (f32[16]{0:T(128)S(1)}, f32[16]{0:T(128)}, u32[]{:S(2)}) copy-start(f32[16]{0:T(128)} %param.29) | copy-start | bytes 196
  5.1 12.1 %copy-start.13 = (s32[8,4]{0,1:T(4,128)S(1)}, s32[8,4]{0,1:T(4,128)}, u32[]{:S(2)}) copy-start(s32[8,4]{0,1:T(4,128)} %param.36) | copy-start | bytes 388
  5.1 12.6 %copy-start.4 = (bf16[2048,16]{0,1:T(8,128)(2,1)S(1)}, bf16[2048,16]{0,1:T(8,128)(2,1)}, u32[]{:S(2)}) copy-start(bf16[2048,16]{0,1:T(8,128)(2,1)} %param.28) | copy-start | bytes 196612
  5.1 12.8 %copy-start.5 = (bf16[2048,16]{0,1:T(8,128)(2,1)S(1)}, bf16[2048,16]{0,1:T(8,128)(2,1)}, u32[]{:S(2)}) copy-start(bf16[2048,16]{0,1:T(8,128)(2,1)} %param.27) | copy-start | bytes 196612
  5.1 12.8 %copy-start.14 = (f32[16]{0:T(128)S(1)}, f32[16]{0:T(128)}, u32[]{:S(2)}) copy-start(f32[16]{0:T(128)} %param.30) | copy-start | bytes 196
  5.1 12.9 %copy-start.6 = (bf16[2048,16]{0,1:T(8,128)(2,1)S(1)}, bf16[2048,16]{0,1:T(8,128)(2,1)}, u32[]{:S(2)}) copy-start(bf16[2048,16]{0,1:T(8,128)(2,1)} %param.26) | copy-start | bytes 196612
  5.1 12.9 %copy-start.7 = (bf16[2048,16]{0,1:T(8,128)(2,1)S(1)}, bf16[2048,16]{0,1:T(8,128)(2,1)}, u32[]{:S(2)}) copy-start(bf16[2048,16]{0,1:T(8,128)(2,1)} %param.25) | copy-start | bytes 196612
  5.1 12.9 %copy-start.8 = (bf16[2048,16]{0,1:T(8,128)(2,1)S(1)}, bf16[2048,16]{0,1:T(8,128)(2,1)}, u32[]{:S(2)}) copy-start(bf16[2048,16]{0,1:T(8,128)(2,1)} %param.24) | copy-start | bytes 196612
  5.1 12.9 %copy-start.9 = (bf16[2048,16]{0,1:T(8,128)(2,1)S(1)}, bf16[2048,16]{0,1:T(8,128)(2,1)}, u32[]{:S(2)}) copy-start(bf16[2048,16]{0,1:T(8,128)(2,1)} %param.23) | copy-start | bytes 196612
  5.1 64.5 %all-to-all-start = ((bf16[128,8,2048]{2,1,0:T(8,128)(2,1)}), bf16[128,8,2048]{2,1,0:T(8,128)(2,1)}, u32[]{:S(2)}, u32[]{:S(2)}) async-start(bf16[128,8,2048]{2,1,0:T(8,128)(2,1)} %stack.12), calls=%async_computation | async-start | bytes 8388608 | tf_op jit(solution)/shard_map/all_to_all | solution.py:17
  75.5 14.5 %all-to-all-start.1 = ((bf16[128,2,256]{2,1,0:T(2,128)(2,1)}), bf16[128,2,256]{2,1,0:T(2,128)(2,1)S(1)}, u32[]{:S(2)}, u32[]{:S(2)}) async-start(bf16[128,2,256]{2,1,0:T(2,128)(2,1)} %reshape.133), calls=%async_computation.1 | async-start | bytes 262144 | tf_op jit(solution)/shard_map/all_to_all | solution.py:93
  92.9 4.0 %copy-start.1 = (bf16[8,16,128,128]{3,2,1,0:T(8,128)(2,1)S(1)}, bf16[8,16,128,128]{3,2,1,0:T(8,128)(2,1)}, u32[]{:S(2)}) copy-start(bf16[8,16,128,128]{3,2,1,0:T(8,128)(2,1)} %param.34) | copy-start | bytes 12582916
  96.9 3.9 %copy-start.15 = (f32[128]{0:T(128)S(1)}, f32[128]{0:T(128)}, u32[]{:S(2)}) copy-start(f32[128]{0:T(128)} %param.31) | copy-start | bytes 1540
  100.9 4.8 %copy-start.2 = (bf16[8,2048]{1,0:T(8,128)(2,1)S(1)}, bf16[8,2048]{1,0:T(8,128)(2,1)}, u32[]{:S(2)}) copy-start(bf16[8,2048]{1,0:T(8,128)(2,1)} %param.21) | copy-start | bytes 98308
  100.9 4.8 %copy-start.3 = (f32[2048]{0:T(1024)S(1)}, f32[2048]{0:T(1024)}, u32[]{:S(2)}) copy-start(f32[2048]{0:T(1024)} %param.33) | copy-start | bytes 24580
  100.9 5.0 %copy-start.10 = (f32[2048]{0:T(1024)S(1)}, f32[2048]{0:T(1024)}, u32[]{:S(2)}) copy-start(f32[2048]{0:T(1024)} %param.35) | copy-start | bytes 24580
  105.7 6.6 %copy-start.11 = (f32[8,4]{0,1:T(4,128)S(1)}, f32[8,4]{0,1:T(4,128)}, u32[]{:S(2)}) copy-start(f32[8,4]{0,1:T(4,128)} %param.37) | copy-start | bytes 388
  108.0 23.4 %all-to-all-start.2 = ((bf16[128,2,2048]{2,1,0:T(2,128)(2,1)}), bf16[128,2,2048]{2,1,0:T(2,128)(2,1)S(1)}, u32[]{:S(2)}, u32[]{:S(2)}) async-start(bf16[128,2,2048]{2,1,0:T(2,128)(2,1)} %bitcast.26), calls=%async_computation.2 | async-start | bytes 2097152 | tf_op jit(solution)/shard_map/all_to_all | solution.py:121
  141.0 23.8 %all-to-all-start.3 = ((bf16[128,2,2048]{2,1,0:T(2,128)(2,1)}), bf16[128,2,2048]{2,1,0:T(2,128)(2,1)S(1)}, u32[]{:S(2)}, u32[]{:S(2)}) async-start(bf16[128,2,2048]{2,1,0:T(2,128)(2,1)} %reshape.118), calls=%async_computation.3 | async-start | bytes 2097152 | tf_op jit(solution)/shard_map/all_to_all | solution.py:128
  145.7 20.4 %copy-start.12 = (f32[2048]{0:T(1024)S(1)}, f32[2048]{0:T(1024)}, u32[]{:S(2)}) copy-start(f32[2048]{0:T(1024)} %param.41) | copy-start | bytes 24580
